TPU v7x, 32 devices: a whole 2x2x4 slice. The times are simulated.
32 devices in a mesh: gr: 2 (over x), sp: 8 (over z, y), tp: 2 (over core).
Axes of the slice: x: 2, y: 2, z: 4, core: 2. Of those that a mesh axis runs over, the one named last changes fastest.
Arguments:
- inputs: bfloat16 [4096, 2048], P(('gr', 'sp'), 'tp'), parts along dimension 0, may hold values from -6 to 6
- x_weight: bfloat16 [2048, 4096], P(None, 'tp'), may hold values from -0.125 to 0.125
- b_weight: bfloat16 [2048, 2048], P(None, 'tp'), may hold values from -0.125 to 0.125
- dt_weight: bfloat16 [2048, 128], replicated, may hold values from -0.125 to 0.125
- dt_bias: float32 [2, 64], replicated, may hold values from -2 to -1
- decay_rate: float32 [2, 64], replicated, may hold values from 0.3 to 10
- conv_x: bfloat16 [5, 4096], P(None, 'tp'), may hold values from -2.5 to 2.5
- conv_b: bfloat16 [5, 2048], P(None, 'tp'), may hold values from -2.5 to 2.5
- query_c: bfloat16 [2, 16, 128], P('gr', 'tp'), parts along dimension 0, may hold values from -6 to 6
- query_gate: bfloat16 [2, 64, 64], P('gr', 'tp'), parts along dimension 0, may hold values from -6 to 6
- read_span: int32 [2], P('gr'), parts along dimension 0, may hold values from 0 to 15
- read_gain: float32 [64, 64], P('tp'), may hold values from 0.1 to 1.9
Outputs:
- span_cache: bfloat16 [32, 2, 64, 8192], P('gr', None, 'tp', 'sp'), parts along dimension 0
- first_read: bfloat16 [2, 64, 64], P('gr', 'tp'), parts along dimension 0
There are 2 independent parts, one for each index of `gr`. A program takes and returns all parts, laid end to end along the dimension named above; an argument that names none is the same for every part. Nothing has to cross between parts.
Inputs may be any that keep to these rules, and one draw needn't show every extreme that they name: read_span holds one span index from 0 to 15.
All inputs are finite; a program needn't handle non-finite values.
Results may differ from a plain program's by a relative error of at most 0.009.
Values may be sent and summed in bfloat16 or wider, within the bound.
A program may use at most 64 MiB of HBM per device.

v0:
```python
import jax
import jax.numpy as jnp
from jax import lax
from jax.sharding import PartitionSpec as P

H = 64
P_SIZE = 64
G = 16
N = 128
KW = 5
SPAN = 128
EPSILON = 1e-06


def extended(shard, sides, width):
    for axis, dim in sides:
        size, length = (lax.axis_size(axis), shard.shape[dim])
        up = [(i, (i + 1) % size) for i in range(size - 1)]
        down = [(j, i) for i, j in up]
        last = lax.slice_in_dim(shard, length - width, length, axis=dim)
        initial = lax.slice_in_dim(shard, 0, width, axis=dim)
        before = lax.ppermute(last, axis, up)
        after = lax.ppermute(initial, axis, down)
        shard = jnp.concatenate([before, shard, after], axis=dim)
    return shard


def span_states(value_rows, key_rows, step_sizes, log_decay):
    running = jnp.cumsum(log_decay, axis=1)
    closing = running[:, -1]
    forward = jnp.exp(closing[:, None, 0] - running[:, :, 0]) * step_sizes[:, :, 0]
    backward = jnp.exp(running[:, :, 1] - log_decay[:, :, 1]) * step_sizes[:, :, 1]
    weights = jnp.stack([forward, backward], axis=2)
    states = jnp.einsum(
        "kseh,kshn,kshp->kehnp",
        weights,
        key_rows.astype(jnp.float32),
        value_rows.astype(jnp.float32),
    )
    return (states, closing)


def read_weights(span_logs, chosen):
    span_count = span_logs.shape[0]
    ahead_sum = jnp.cumsum(span_logs[:, 0], axis=0)
    behind = jnp.flip(jnp.cumsum(jnp.flip(span_logs[:, 1], 0), axis=0), 0)
    positions = jnp.arange(span_count, dtype=jnp.int32)[:, None]
    ahead_pick = lax.dynamic_slice_in_dim(ahead_sum, chosen, 1, 0)
    behind_pick = lax.dynamic_slice_in_dim(behind, chosen, 1, 0)
    before = positions <= chosen
    after = positions >= chosen
    forward = jnp.where(before, jnp.exp(jnp.where(before, ahead_pick - ahead_sum, 0.0)), 0.0)
    backward = jnp.where(after, jnp.exp(jnp.where(after, behind_pick - behind, 0.0)), 0.0)
    return jnp.stack([forward, backward], axis=1)


def per_device(
    inputs,
    x_weight,
    b_weight,
    dt_weight,
    dt_bias,
    decay_rate,
    conv_x,
    conv_b,
    query_c,
    query_gate,
    read_span,
    read_gain,
):
    tokens = inputs.shape[0]
    heads_local = x_weight.shape[1] // P_SIZE
    per_group = H // G
    tp_index = lax.axis_index("tp")
    sp_index = lax.axis_index("sp")
    dt_local = lax.dynamic_slice_in_dim(
        dt_weight.reshape(dt_weight.shape[0], 2, H), tp_index * heads_local, heads_local, 2
    )
    dt_local = dt_local.reshape(dt_weight.shape[0], 2 * heads_local)
    slab_piece = lax.all_gather(inputs, "tp", axis=1, tiled=True)
    x_part = jnp.dot(slab_piece, x_weight, preferred_element_type=jnp.float32)
    b_part = jnp.dot(slab_piece, b_weight, preferred_element_type=jnp.float32)
    dt_part = jnp.dot(slab_piece, dt_local, preferred_element_type=jnp.float32)
    joined = jnp.concatenate([x_part.astype(jnp.bfloat16), b_part.astype(jnp.bfloat16)], axis=1)
    reach = KW // 2
    padded = extended(joined, (("sp", 0),), reach)
    taps = jnp.concatenate([conv_x, conv_b], axis=1)
    mixed_rows = jnp.zeros(joined.shape, jnp.float32)
    for offset in range(KW):
        mixed_rows = mixed_rows + taps[offset].astype(jnp.float32) * padded[
            offset : offset + tokens
        ].astype(jnp.float32)
    mixed_rows = jax.nn.silu(mixed_rows).astype(jnp.bfloat16)
    split_at = x_weight.shape[1]
    values = mixed_rows[:, :split_at]
    key_rows = mixed_rows[:, split_at:]
    length = tokens * lax.axis_size("sp")
    bias_local = lax.dynamic_slice_in_dim(dt_bias, tp_index * heads_local, heads_local, 1)
    rate_local = lax.dynamic_slice_in_dim(decay_rate, tp_index * heads_local, heads_local, 1)
    dt_raw = dt_part.astype(jnp.bfloat16).reshape(tokens, 2, heads_local)
    step_sizes = jax.nn.softplus(dt_raw.astype(jnp.float32) + bias_local)
    log_decay = -(step_sizes * rate_local) / length
    span_count = tokens // SPAN
    value_rows = values.reshape(span_count, SPAN, heads_local, P_SIZE)
    group_keys = key_rows.reshape(span_count, SPAN, heads_local // per_group, N)
    group_keys = jnp.repeat(group_keys, per_group, axis=2)
    states, closing = span_states(
        value_rows,
        group_keys,
        step_sizes.reshape(span_count, SPAN, 2, heads_local),
        log_decay.reshape(span_count, SPAN, 2, heads_local),
    )
    local_rows = states.reshape(span_count, 2, heads_local, N * P_SIZE).astype(jnp.bfloat16)
    all_logs = lax.all_gather(closing, "sp", axis=0, tiled=True)
    weights = read_weights(all_logs, read_span[0])
    cache_rows = lax.all_to_all(local_rows, "sp", split_axis=3, concat_axis=0, tiled=True)
    columns = cache_rows.shape[3] // P_SIZE
    gathered = jnp.einsum("jeh,jehx->hx", weights, cache_rows.astype(jnp.float32)).reshape(
        heads_local, columns, P_SIZE
    )
    picked = lax.dynamic_slice_in_dim(query_c[0], sp_index * columns, columns, 1)
    query_cols = jnp.repeat(picked.astype(jnp.float32), per_group, axis=0)
    partial_read = jnp.einsum("hnp,hn->hp", gathered, query_cols)
    read_total = lax.psum(partial_read, "sp")
    gated_read = read_total * jax.nn.silu(query_gate[0].astype(jnp.float32))
    square_sum = lax.psum(jnp.sum(gated_read * gated_read), "tp")
    mean_square = square_sum / (H * P_SIZE)
    first_read = (gated_read * lax.rsqrt(mean_square + EPSILON) * read_gain)[None].astype(
        jnp.bfloat16
    )
    return (cache_rows, first_read)


def solution(mesh):
    return jax.shard_map(
        per_device,
        mesh=mesh,
        in_specs=(
            P(("gr", "sp"), "tp"),
            P(None, "tp"),
            P(None, "tp"),
            P(),
            P(),
            P(),
            P(None, "tp"),
            P(None, "tp"),
            P("gr", "tp", None),
            P("gr", "tp", None),
            P("gr"),
            P("tp", None),
        ),
        out_specs=(P("gr", None, "tp", "sp"), P("gr", "tp", None)),
        check_vma=False,
    )
```

profile of v0, /device:TPU:0, one launch (start us, length us, event | category | flops | bytes accessed | tf_op | source)
XLA Modules:
  0.0 222.9 jit_solution(17773302501208012883)
XLA Ops:
  7.2 0.7 all-gather.3.cloned.1.call-update
  7.9 0.8 constant_dynamic-update-slice_fusion.1
  8.7 0.8 constant_dynamic-slice_fusion.2
  9.4 1.2 copy.63
  10.7 0.7 constant_dynamic-update-slice_fusion
  11.5 9.8 %all-gather.3.cloned.1.call-done = bf16[256,2048]{1,0:T(8,128)(2,1)} async-done(((bf16[256,1024]{1,0:T(8,128)(2,1)}), bf16[256,2048]{1,0:T(8,128)(2,1)}) %all-gather.3.cloned.1.call-update) | async-done | bytes 1048592 | tf_op jit(solution)/shard_map/all_gather | solution.py:80
  21.3 1.8 fusion.9
  23.2 0.2 copy.65
  23.5 0.2 fusion.24
  23.9 5.9 %convolution_convert_fusion = bf16[256,2048]{1,0:T(8,128)(2,1)S(1)} fusion(bf16[256,2048]{1,0:T(8,128)(2,1)S(1)} %copy-done.1, bf16[2048,2048]{1,0:T(8,128)(2,1)} %param.13), kind=kOutput, calls=%fused_computation.3 | convolution fusion | flops 2148007936 | bytes 10485760 | tf_op jit(solution)/shard_map/dot_general | solution.py:81
  29.8 1.3 convolution_convert_fusion.1
  31.1 3.6 %collective-permute-start = (bf16[2,3072]{1,0:T(2,128)(2,1)S(1)}, bf16[2,3072]{1,0:T(2,128)(2,1)S(1)}, u32[]{:S(2)}, u32[]{:S(2)}) collective-permute-start(bf16[2,3072]{1,0:T(2,128)(2,1)S(1)} %get-tuple-element.6), channel_id=1, source_target_pairs={{0,2},{2,4},{4,6},{6,8},{8,10},{10,12},{12,14},{1,3},{3,5},{5,7},{... | collective-permute-start | bytes 36872 | tf_op jit(solution)/shard_map/ppermute | solution.py:22
  34.8 1.3 collective-permute-start.1
  36.3 4.1 %collective-permute-done.1 = bf16[2,3072]{1,0:T(2,128)(2,1)S(1)} collective-permute-done((bf16[2,3072]{1,0:T(2,128)(2,1)S(1)}, bf16[2,3072]{1,0:T(2,128)(2,1)S(1)}, u32[]{:S(2)}, u32[]{:S(2)}) %collective-permute-start.1) | collective-permute-done | bytes 12320 | tf_op jit(solution)/shard_map/ppermute | solution.py:23
  40.4 0.5 maximum_maximum_fusion
  40.9 2.9 %multiply_convert_fusion = bf16[256,3072]{1,0:T(8,128)(2,1)S(1)} fusion(bf16[256,1024]{1,0:T(8,128)(2,1)S(1)} %convolution_convert_fusion.1, bf16[256,2048]{1,0:T(8,128)(2,1)S(1)} %convolution_convert_fusion, bf16[258,3072]{1,0:T(8,128)(2,1)S(1)} %get-tuple-element.5, bf16[258,3072]{1,0:T(8,128)(2,1)S(1)} %get-tuple-element.4, f32[3072]{0:T(1024)S(1)} %bitcast.103, ...), kind=kLoop, calls=%fused_computation.2 | loop fusion | flops 17301504 | bytes 9498624 | tf_op jit(solution)/shard_map/convert_element_type | solution.py:93
  43.7 0.2 slice_convert_fusion
  44.0 3.0 %reshape.152 = f32[2,128,32,64]{3,2,1,0:T(8,128)} reshape(f32[256,2048]{1,0:T(8,128)S(1)} %slice_convert_fusion) | data formatting | bytes 4194304 | tf_op jit(solution)/shard_map/convert.7
  47.0 3.8 %copy.62 = f32[2,128,32,64]{1,3,2,0:T(8,128)S(1)} copy(f32[2,128,32,64]{3,2,1,0:T(8,128)} %reshape.152) | data formatting | bytes 4194304 | tf_op jit(solution)/shard_map/convert.7
  51.0 0.6 broadcast_in_dim.43
  51.6 2.0 convert_bitcast_fusion
  53.6 14.1 %copy.82 = bf16[2,2,32,128,64]{2,1,0,4,3:T(2,128)(2,1)} copy(bf16[2,2,32,128,64]{3,4,1,2,0:T(8,128)(2,1)} %convert_bitcast_fusion) | data formatting | bytes 4194304 | tf_op jit(solution)/shard_map/convert_element_type | solution.py:113
  67.7 11.2 %reshape.153 = bf16[8,2,65536]{2,1,0:T(2,128)(2,1)} reshape(bf16[8192,2,2,32]{3,2,1,0:T(2,128)(2,1)} %bitcast.92) | data formatting | bytes 4194304
  78.9 5.6 %all-to-all-start = ((bf16[8,2,65536]{2,1,0:T(2,128)(2,1)}), bf16[8,2,65536]{2,1,0:T(2,128)(2,1)S(1)}, u32[]{:S(2)}, u32[]{:S(2)}) async-start(bf16[8,2,65536]{2,1,0:T(2,128)(2,1)} %reshape.153), calls=%async_computation | async-start | bytes 4194304 | tf_op jit(solution)/shard_map/all_to_all | solution.py:116
  85.2 65.2 %all-gather = f32[16,1,2,32]{3,2,1,0:T(2,128)S(1)} all-gather(f32[2,1,2,32]{3,2,1,0:T(2,128)S(1)} %get-tuple-element.8), channel_id=2, replica_groups=mesh['gr'=2,'sp'=8,'tp'=2] {'sp'}, dimensions={0}, use_global_device_ids=true | all-gather | bytes 4608 | tf_op jit(solution)/shard_map/all_gather | solution.py:114
  150.8 6.6 %reshape.154 = bf16[8192,2,2,32]{3,2,1,0:T(2,128)(2,1)} reshape(bf16[8,2,65536]{2,1,0:T(2,128)(2,1)S(1)} %all-to-all-done) | data formatting | bytes 4194304
  157.4 17.8 %copy.84 = bf16[2,2,32,8,1024]{4,2,1,0,3:T(8,128)(2,1)S(1)} copy(bf16[2,2,32,8,1024]{2,1,0,4,3:T(2,128)(2,1)} %bitcast.93) | data formatting | bytes 4194304 | tf_op jit(solution)/shard_map/all_to_all | solution.py:116
  175.2 2.4 %fusion.2 = bf16[32,1,1024,1]{2,1,3,0:T(2,128)(2,1)S(1)} fusion(bf16[16,2,32,1]{0,3,1,2:T(2,128)(2,1)S(1)} %copy.75, bf16[16,2,32,1024]{3,2,1,0:T(8,128)(2,1)S(1)} %bitcast.95), kind=kOutput, calls=%fused_computation.7 | convolution fusion | flops 2097152 | bytes 2164736 | tf_op jit(solution)/shard_map/jeh,jehx->hx/dot_general | solution.py:118
  178.0 33.1 %psum.14 = f32[32,64]{1,0:T(8,128)S(1)} all-reduce(f32[32,64]{1,0:T(8,128)S(1)} %bitcast.110), channel_id=1, replica_groups=mesh['gr'=2,'sp'=8,'tp'=2] {'sp'}, use_global_device_ids=true, to_apply=%region_3.4 | all-reduce | flops 2048 | bytes 16384 | tf_op jit(solution)/shard_map/psum | solution.py:124
  211.0 0.6 multiply_reduce_fusion
  211.7 3.1 %psum.15 = f32[]{:T(128)} all-reduce(f32[]{:T(128)} %multiply_reduce_fusion), channel_id=1, replica_groups=mesh['gr'=2,'sp'=8,'tp'=2] {'tp'}, use_global_device_ids=true, to_apply=%region_5.6 | all-reduce | flops 1 | bytes 8 | tf_op jit(solution)/shard_map/psum | solution.py:126
  215.4 0.6 fusion.17
  (48 shorter events, 1.8 us)
Async XLA Ops:
  7.2 14.1 %all-gather.3.cloned.1.call-start = ((), (), s32[]{:S(2)}) async-start(), calls=%async_computation.1 | async-start | bytes 1572864 | tf_op jit(solution)/shard_map/all_gather | solution.py:80
  21.3 2.6 %copy-start.1 = (bf16[256,2048]{1,0:T(8,128)(2,1)S(1)}, bf16[256,2048]{1,0:T(8,128)(2,1)}, u32[]{:S(2)}) copy-start(bf16[256,2048]{1,0:T(8,128)(2,1)} %all-gather.3.cloned.1.call-done) | copy-start | bytes 3145732
  23.9 5.9 %copy-start.5 = (bf16[2048,1024]{1,0:T(8,128)(2,1)S(1)}, bf16[2048,1024]{1,0:T(8,128)(2,1)}, u32[]{:S(2)}) copy-start(bf16[2048,1024]{1,0:T(8,128)(2,1)} %param.14) | copy-start | bytes 12582916
  31.1 5.1 %collective-permute-start = (bf16[2,3072]{1,0:T(2,128)(2,1)S(1)}, bf16[2,3072]{1,0:T(2,128)(2,1)S(1)}, u32[]{:S(2)}, u32[]{:S(2)}) collective-permute-start(bf16[2,3072]{1,0:T(2,128)(2,1)S(1)} %get-tuple-element.6), channel_id=1, source_target_pairs={{0,2},{2,4},{4,6},{6,8},{8,10},{10,12},{12,14},{1,3},{3,5},{5,7},{... | collective-permute-start | bytes 36872 | tf_op jit(solution)/shard_map/ppermute | solution.py:22
  34.8 5.6 %collective-permute-start.1 = (bf16[2,3072]{1,0:T(2,128)(2,1)S(1)}, bf16[2,3072]{1,0:T(2,128)(2,1)S(1)}, u32[]{:S(2)}, u32[]{:S(2)}) collective-permute-start(bf16[2,3072]{1,0:T(2,128)(2,1)S(1)} %get-tuple-element.7), channel_id=1, source_target_pairs={{2,0},{4,2},{6,4},{8,6},{10,8},{12,10},{14,12},{3,1},{5,3},{7,5},{... | collective-permute-start | bytes 36872 | tf_op jit(solution)/shard_map/ppermute | solution.py:23
  78.8 6.3 %copy-start.4 = (bf16[1,8,128]{2,1,0:T(8,128)(2,1)S(1)}, bf16[1,8,128]{2,1,0:T(8,128)(2,1)}, u32[]{:S(2)}) copy-start(bf16[1,8,128]{2,1,0:T(8,128)(2,1)} %param.20) | copy-start | bytes 6148
  78.9 72.0 %all-to-all-start = ((bf16[8,2,65536]{2,1,0:T(2,128)(2,1)}), bf16[8,2,65536]{2,1,0:T(2,128)(2,1)S(1)}, u32[]{:S(2)}, u32[]{:S(2)}) async-start(bf16[8,2,65536]{2,1,0:T(2,128)(2,1)} %reshape.153), calls=%async_computation | async-start | bytes 4194304 | tf_op jit(solution)/shard_map/all_to_all | solution.py:116
  157.4 53.7 %copy-start.2 = (bf16[1,32,64]{2,1,0:T(8,128)(2,1)S(1)}, bf16[1,32,64]{2,1,0:T(8,128)(2,1)}, u32[]{:S(2)}) copy-start(bf16[1,32,64]{2,1,0:T(8,128)(2,1)} %param.21) | copy-start | bytes 12292
  175.2 40.9 %copy-start = (bf16[2,2,32,8,1024]{4,2,1,0,3:T(8,128)(2,1)}, bf16[2,2,32,8,1024]{4,2,1,0,3:T(8,128)(2,1)S(1)}, u32[]{:S(2)}) copy-start(bf16[2,2,32,8,1024]{4,2,1,0,3:T(8,128)(2,1)S(1)} %copy.84) | copy-start | bytes 6291460
  175.2 40.2 %copy-start.3 = (f32[32,64]{1,0:T(8,128)S(1)}, f32[32,64]{1,0:T(8,128)}, u32[]{:S(2)}) copy-start(f32[32,64]{1,0:T(8,128)} %param.23) | copy-start | bytes 24580
Sparse Core Ops, SparseCore 0:
  9.5 11.7 all-gather.2
where the time goes:
time: 224 us; the launch traced here: 223 us
  blocking collectives  101 us (45%)
  local copies, waits for them, and re-layouts  61.6 us (28%)
  between operations  15.7 us (7%)
  waiting for transfers between devices  14.6 us (7%)
  matrix products  13.5 us (6%)
  starting transfers between devices  10.6 us (5%)
  other arithmetic  5.54 us (2%)
    all_gather x1, blocking collectives, per_device(): all_logs = lax.all_gather(closing, 'sp', axis=0, tiled=True)  65.2 us
    psum x1, blocking collectives, per_device(): read_total = lax.psum(partial_read, 'sp')  33.1 us
    unnamed x20, local copies, waits for them, and re-layouts  20.1 us
    all_to_all x1, local copies, waits for them, and re-layouts, per_device(): lax.all_to_all(local_rows, 'sp', split_axis=3, concat_axis=0, tiled=True)  17.8 us
    convert_element_type x1, local copies, waits for them, and re-layouts, per_device(): states.reshape(span_count, 2, heads_local, N * P_SIZE).astype(jnp.bfloat16)  14.1 us
    all_gather x1, waiting for transfers between devices, per_device(): slab_piece = lax.all_gather(inputs, 'tp', axis=1, tiled=True)  9.82 us
    another operation x2, local copies, waits for them, and re-layouts  6.77 us
    dot_general x1, matrix products, per_device(): x_part = jnp.dot(slab_piece, x_weight, preferred_element_type=jnp.float32)  5.86 us
  transfers between devices with their start and end apart: 4, of which 2 were waited for; matrix products, arithmetic and copies ran while one was open for 2% of the time, Pallas kernels for 0%

commit v1 on v0

--- a/solution.py
+++ b/solution.py
@@ -121,7 +121,7 @@
     picked = lax.dynamic_slice_in_dim(query_c[0], sp_index * columns, columns, 1)
     query_cols = jnp.repeat(picked.astype(jnp.float32), per_group, axis=0)
     partial_read = jnp.einsum("hnp,hn->hp", gathered, query_cols)
-    read_total = lax.psum(partial_read, "sp")
+    read_total = lax.all_gather(partial_read, "sp").sum(axis=0)
     gated_read = read_total * jax.nn.silu(query_gate[0].astype(jnp.float32))
     square_sum = lax.psum(jnp.sum(gated_read * gated_read), "tp")
     mean_square = square_sum / (H * P_SIZE)

time: 224 us -> 222 us (level)
    psum x1 -> x0, blocking collectives: 33.1 us -> none  [per_device(): read_total = lax.psum(partial_read, 'sp')]
    all_gather x0 -> x1, blocking collectives: none -> 30.5 us  [per_device(): read_total = lax.all_gather(partial_read, 'sp').sum(axis=0)]
where the time goes in v1:
time: 222 us; the launch traced here: 220 us
  blocking collectives  98.8 us (45%)
  local copies, waits for them, and re-layouts  61.6 us (28%)
  between operations  15.7 us (7%)
  waiting for transfers between devices  14.6 us (7%)
  matrix products  13.5 us (6%)
  starting transfers between devices  10.6 us (5%)
  other arithmetic  5.56 us (3%)
    all_gather x1, blocking collectives, per_device(): all_logs = lax.all_gather(closing, 'sp', axis=0, tiled=True)  65.2 us
    all_gather x1, blocking collectives, per_device(): read_total = lax.all_gather(partial_read, 'sp').sum(axis=0)  30.5 us
    unnamed x20, local copies, waits for them, and re-layouts  20.1 us
    all_to_all x1, local copies, waits for them, and re-layouts, per_device(): lax.all_to_all(local_rows, 'sp', split_axis=3, concat_axis=0, tiled=True)  17.8 us
    convert_element_type x1, local copies, waits for them, and re-layouts, per_device(): states.reshape(span_count, 2, heads_local, N * P_SIZE).astype(jnp.bfloat16)  14.1 us
    all_gather x1, waiting for transfers between devices, per_device(): slab_piece = lax.all_gather(inputs, 'tp', axis=1, tiled=True)  9.82 us
    another operation x2, local copies, waits for them, and re-layouts  6.77 us
    dot_general x1, matrix products, per_device(): x_part = jnp.dot(slab_piece, x_weight, preferred_element_type=jnp.float32)  5.86 us
  transfers between devices with their start and end apart: 4, of which 2 were waited for; matrix products, arithmetic and copies ran while one was open for 2% of the time, Pallas kernels for 0%

profile of v1, /device:TPU:0, one launch (start us, length us, event | category | flops | bytes accessed | tf_op | source)
XLA Modules:
  0.0 220.4 jit_solution(2304580302520683202)
XLA Ops:
  7.2 0.7 all-gather.4.cloned.1.call-update
  7.9 0.8 constant_dynamic-update-slice_fusion.1
  8.7 0.8 constant_dynamic-slice_fusion.2
  9.4 1.2 copy.79
  10.7 0.7 constant_dynamic-update-slice_fusion
  11.5 9.8 %all-gather.4.cloned.1.call-done = bf16[256,2048]{1,0:T(8,128)(2,1)} async-done(((bf16[256,1024]{1,0:T(8,128)(2,1)}), bf16[256,2048]{1,0:T(8,128)(2,1)}) %all-gather.4.cloned.1.call-update) | async-done | bytes 1048592 | tf_op jit(solution)/shard_map/all_gather | solution.py:80
  21.3 1.8 fusion.9
  23.2 0.2 copy.81
  23.5 0.2 fusion.24
  23.9 5.9 %convolution_convert_fusion = bf16[256,2048]{1,0:T(8,128)(2,1)S(1)} fusion(bf16[256,2048]{1,0:T(8,128)(2,1)S(1)} %copy-done.1, bf16[2048,2048]{1,0:T(8,128)(2,1)} %param.13), kind=kOutput, calls=%fused_computation.3 | convolution fusion | flops 2148007936 | bytes 10485760 | tf_op jit(solution)/shard_map/dot_general | solution.py:81
  29.8 1.3 convolution_convert_fusion.1
  31.1 3.6 %collective-permute-start = (bf16[2,3072]{1,0:T(2,128)(2,1)S(1)}, bf16[2,3072]{1,0:T(2,128)(2,1)S(1)}, u32[]{:S(2)}, u32[]{:S(2)}) collective-permute-start(bf16[2,3072]{1,0:T(2,128)(2,1)S(1)} %get-tuple-element.6), channel_id=1, source_target_pairs={{0,2},{2,4},{4,6},{6,8},{8,10},{10,12},{12,14},{1,3},{3,5},{5,7},{... | collective-permute-start | bytes 36872 | tf_op jit(solution)/shard_map/ppermute | solution.py:22
  34.8 1.3 collective-permute-start.1
  36.3 4.1 %collective-permute-done.1 = bf16[2,3072]{1,0:T(2,128)(2,1)S(1)} collective-permute-done((bf16[2,3072]{1,0:T(2,128)(2,1)S(1)}, bf16[2,3072]{1,0:T(2,128)(2,1)S(1)}, u32[]{:S(2)}, u32[]{:S(2)}) %collective-permute-start.1) | collective-permute-done | bytes 12320 | tf_op jit(solution)/shard_map/ppermute | solution.py:23
  40.4 0.5 maximum_maximum_fusion
  40.9 2.9 %multiply_convert_fusion = bf16[256,3072]{1,0:T(8,128)(2,1)S(1)} fusion(bf16[256,1024]{1,0:T(8,128)(2,1)S(1)} %convolution_convert_fusion.1, bf16[256,2048]{1,0:T(8,128)(2,1)S(1)} %convolution_convert_fusion, bf16[258,3072]{1,0:T(8,128)(2,1)S(1)} %get-tuple-element.5, bf16[258,3072]{1,0:T(8,128)(2,1)S(1)} %get-tuple-element.4, f32[3072]{0:T(1024)S(1)} %bitcast.105, ...), kind=kLoop, calls=%fused_computation.2 | loop fusion | flops 17301504 | bytes 9498624 | tf_op jit(solution)/shard_map/convert_element_type | solution.py:93
  43.7 0.2 slice_convert_fusion
  44.0 3.0 %reshape.153 = f32[2,128,32,64]{3,2,1,0:T(8,128)} reshape(f32[256,2048]{1,0:T(8,128)S(1)} %slice_convert_fusion) | data formatting | bytes 4194304 | tf_op jit(solution)/shard_map/convert.7
  47.0 3.8 %copy.78 = f32[2,128,32,64]{1,3,2,0:T(8,128)S(1)} copy(f32[2,128,32,64]{3,2,1,0:T(8,128)} %reshape.153) | data formatting | bytes 4194304 | tf_op jit(solution)/shard_map/convert.7
  51.0 0.6 broadcast_in_dim.43
  51.6 2.0 convert_bitcast_fusion
  53.6 14.1 %copy.98 = bf16[2,2,32,128,64]{2,1,0,4,3:T(2,128)(2,1)} copy(bf16[2,2,32,128,64]{3,4,1,2,0:T(8,128)(2,1)} %convert_bitcast_fusion) | data formatting | bytes 4194304 | tf_op jit(solution)/shard_map/convert_element_type | solution.py:113
  67.7 11.2 %reshape.154 = bf16[8,2,65536]{2,1,0:T(2,128)(2,1)} reshape(bf16[8192,2,2,32]{3,2,1,0:T(2,128)(2,1)} %bitcast.93) | data formatting | bytes 4194304
  78.9 5.6 %all-to-all-start = ((bf16[8,2,65536]{2,1,0:T(2,128)(2,1)}), bf16[8,2,65536]{2,1,0:T(2,128)(2,1)S(1)}, u32[]{:S(2)}, u32[]{:S(2)}) async-start(bf16[8,2,65536]{2,1,0:T(2,128)(2,1)} %reshape.154), calls=%async_computation | async-start | bytes 4194304 | tf_op jit(solution)/shard_map/all_to_all | solution.py:116
  85.2 65.2 %all-gather = f32[16,1,2,32]{3,2,1,0:T(2,128)S(1)} all-gather(f32[2,1,2,32]{3,2,1,0:T(2,128)S(1)} %get-tuple-element.8), channel_id=2, replica_groups=mesh['gr'=2,'sp'=8,'tp'=2] {'sp'}, dimensions={0}, use_global_device_ids=true | all-gather | bytes 4608 | tf_op jit(solution)/shard_map/all_gather | solution.py:114
  150.8 6.6 %reshape.155 = bf16[8192,2,2,32]{3,2,1,0:T(2,128)(2,1)} reshape(bf16[8,2,65536]{2,1,0:T(2,128)(2,1)S(1)} %all-to-all-done) | data formatting | bytes 4194304
  157.4 17.8 %copy.100 = bf16[2,2,32,8,1024]{4,2,1,0,3:T(8,128)(2,1)S(1)} copy(bf16[2,2,32,8,1024]{2,1,0,4,3:T(2,128)(2,1)} %bitcast.94) | data formatting | bytes 4194304 | tf_op jit(solution)/shard_map/all_to_all | solution.py:116
  175.2 2.4 %fusion.2 = bf16[32,1,1024,1]{2,1,3,0:T(2,128)(2,1)S(1)} fusion(bf16[16,2,32,1]{0,3,1,2:T(2,128)(2,1)S(1)} %copy.91, bf16[16,2,32,1024]{3,2,1,0:T(8,128)(2,1)S(1)} %bitcast.96), kind=kOutput, calls=%fused_computation.7 | convolution fusion | flops 2097152 | bytes 2164736 | tf_op jit(solution)/shard_map/jeh,jehx->hx/dot_general | solution.py:118
  178.0 30.5 %all-gather.1 = f32[256,64]{1,0:T(8,128)S(1)} all-gather(f32[32,64]{1,0:T(8,128)S(1)} %bitcast.111), channel_id=3, replica_groups=mesh['gr'=2,'sp'=8,'tp'=2] {'sp'}, dimensions={0}, use_global_device_ids=true | all-gather | bytes 73728 | tf_op jit(solution)/shard_map/all_gather | solution.py:124
  208.5 0.6 multiply_reduce_fusion
  209.1 3.1 %psum.7 = f32[]{:T(128)} all-reduce(f32[]{:T(128)} %multiply_reduce_fusion), channel_id=1, replica_groups=mesh['gr'=2,'sp'=8,'tp'=2] {'tp'}, use_global_device_ids=true, to_apply=%region_5.6 | all-reduce | flops 1 | bytes 8 | tf_op jit(solution)/shard_map/psum | solution.py:126
  212.9 0.6 fusion.17
  (49 shorter events, 1.8 us)
Async XLA Ops:
  7.2 14.1 %all-gather.4.cloned.1.call-start = ((), (), s32[]{:S(2)}) async-start(), calls=%async_computation.1 | async-start | bytes 1572864 | tf_op jit(solution)/shard_map/all_gather | solution.py:80
  21.3 2.6 %copy-start.1 = (bf16[256,2048]{1,0:T(8,128)(2,1)S(1)}, bf16[256,2048]{1,0:T(8,128)(2,1)}, u32[]{:S(2)}) copy-start(bf16[256,2048]{1,0:T(8,128)(2,1)} %all-gather.4.cloned.1.call-done) | copy-start | bytes 3145732
  23.9 5.9 %copy-start.5 = (bf16[2048,1024]{1,0:T(8,128)(2,1)S(1)}, bf16[2048,1024]{1,0:T(8,128)(2,1)}, u32[]{:S(2)}) copy-start(bf16[2048,1024]{1,0:T(8,128)(2,1)} %param.14) | copy-start | bytes 12582916
  31.1 5.1 %collective-permute-start = (bf16[2,3072]{1,0:T(2,128)(2,1)S(1)}, bf16[2,3072]{1,0:T(2,128)(2,1)S(1)}, u32[]{:S(2)}, u32[]{:S(2)}) collective-permute-start(bf16[2,3072]{1,0:T(2,128)(2,1)S(1)} %get-tuple-element.6), channel_id=1, source_target_pairs={{0,2},{2,4},{4,6},{6,8},{8,10},{10,12},{12,14},{1,3},{3,5},{5,7},{... | collective-permute-start | bytes 36872 | tf_op jit(solution)/shard_map/ppermute | solution.py:22
  34.8 5.6 %collective-permute-start.1 = (bf16[2,3072]{1,0:T(2,128)(2,1)S(1)}, bf16[2,3072]{1,0:T(2,128)(2,1)S(1)}, u32[]{:S(2)}, u32[]{:S(2)}) collective-permute-start(bf16[2,3072]{1,0:T(2,128)(2,1)S(1)} %get-tuple-element.7), channel_id=1, source_target_pairs={{2,0},{4,2},{6,4},{8,6},{10,8},{12,10},{14,12},{3,1},{5,3},{7,5},{... | collective-permute-start | bytes 36872 | tf_op jit(solution)/shard_map/ppermute | solution.py:23
  78.8 6.3 %copy-start.4 = (bf16[1,8,128]{2,1,0:T(8,128)(2,1)S(1)}, bf16[1,8,128]{2,1,0:T(8,128)(2,1)}, u32[]{:S(2)}) copy-start(bf16[1,8,128]{2,1,0:T(8,128)(2,1)} %param.20) | copy-start | bytes 6148
  78.9 72.0 %all-to-all-start = ((bf16[8,2,65536]{2,1,0:T(2,128)(2,1)}), bf16[8,2,65536]{2,1,0:T(2,128)(2,1)S(1)}, u32[]{:S(2)}, u32[]{:S(2)}) async-start(bf16[8,2,65536]{2,1,0:T(2,128)(2,1)} %reshape.154), calls=%async_computation | async-start | bytes 4194304 | tf_op jit(solution)/shard_map/all_to_all | solution.py:116
  175.2 38.4 %copy-start = (bf16[2,2,32,8,1024]{4,2,1,0,3:T(8,128)(2,1)}, bf16[2,2,32,8,1024]{4,2,1,0,3:T(8,128)(2,1)S(1)}, u32[]{:S(2)}) copy-start(bf16[2,2,32,8,1024]{4,2,1,0,3:T(8,128)(2,1)S(1)} %copy.100) | copy-start | bytes 6291460
  175.2 33.3 %copy-start.2 = (bf16[1,32,64]{2,1,0:T(8,128)(2,1)S(1)}, bf16[1,32,64]{2,1,0:T(8,128)(2,1)}, u32[]{:S(2)}) copy-start(bf16[1,32,64]{2,1,0:T(8,128)(2,1)} %param.21) | copy-start | bytes 12292
  175.2 37.7 %copy-start.3 = (f32[32,64]{1,0:T(8,128)S(1)}, f32[32,64]{1,0:T(8,128)}, u32[]{:S(2)}) copy-start(f32[32,64]{1,0:T(8,128)} %param.23) | copy-start | bytes 24580
Sparse Core Ops, SparseCore 0:
  9.5 11.7 all-gather.3
